TPU v7x, 32 devices: a whole 2x2x4 slice. The times are simulated.
32 devices in a mesh: sp: 8 (over z, x), tp: 4 (over y, core).
Axes of the slice: x: 2, y: 2, z: 4, core: 2. Of those that a mesh axis runs over, the one named last changes fastest.
Arguments:
- tokens: bfloat16 [4096, 2048], P(('sp', 'tp')), may hold values from -6 to 6
- norm_gain: float32 [2048], replicated, may hold values from 0.1 to 1.9
- pool_in_weight: bfloat16 [2048, 1024], P('sp', 'tp'), may hold values from -0.125 to 0.125
- query_weight: bfloat16 [2048, 1024], P('sp', 'tp'), may hold values from -0.125 to 0.125
- forget_weight: bfloat16 [2048, 1024], P('sp', 'tp'), may hold values from -0.125 to 0.125
- input_weight: bfloat16 [2048, 1024], P('sp', 'tp'), may hold values from -0.125 to 0.125
- forget_gap: float32 [1024], P('tp'), may hold values from 0 to 0.02
- decay_shift: float32 [8, 4096], P('tp', 'sp'), may hold values from -0.42 to 0
- out_gain: float32 [128], replicated, may hold values from 0.1 to 1.9
- pool_out_weight: bfloat16 [1024, 2048], P('tp', 'sp'), may hold values from -0.53033009 to 0.53033009
- recur_out_weight: bfloat16 [1024, 2048], P('tp', 'sp'), may hold values from -0.53033009 to 0.53033009
Outputs:
- mixed_out: bfloat16 [4096, 2048], P(('sp', 'tp'))
All inputs are finite; a program needn't handle non-finite values.
Results may differ from a plain program's by a relative error of at most 0.014.
Values may be sent and summed in bfloat16 or wider, within the bound.
A program may use at most 64 MiB of HBM per device.

v0:
```python
import jax
import jax.numpy as jnp
from jax import lax
from jax.sharding import PartitionSpec as P

GROUPS = 4
RDIM = 128
SPAN = 64
EPSILON = 1e-06
EXACT_MATMUL = lax.Precision.HIGHEST


def passed_along(block, axis, distance):
    devices = range(lax.axis_size(axis))
    route = [(i - distance, i) for i in devices if i - distance in devices]
    return lax.ppermute(block, axis, route)


def prefix(part, axis, combine, identity):
    place = lax.axis_index(axis)
    gathered = jax.tree.map(lambda a: lax.all_gather(a, axis), part)
    state = jax.tree.map(lambda a, e: jnp.zeros_like(a) + jnp.asarray(e, a.dtype), part, identity)

    def one(hop, state):
        return combine(
            state, jax.tree.map(lambda a: lax.dynamic_index_in_dim(a, hop, 0, False), gathered)
        )

    return lax.fori_loop(0, place, one, state)


def window_sums(padded, levels, reach):
    length = padded.shape[0] - reach
    results = []
    running = padded
    for level in range(levels):
        width = 2**level
        running = running[width:] + running[:-width]
        offset = reach + 1 - 2 * width
        results.append(lax.slice_in_dim(running, offset, offset + length, axis=0))
    return results


def chain(earlier, later):
    return (earlier[0] * later[0], later[0][:, :, None] * earlier[1] + later[1])


def to_blocks(tensor, block_count, head_count):
    return tensor.reshape(block_count, SPAN, head_count, RDIM).transpose(0, 2, 1, 3)


def local(
    tokens,
    norm_gain,
    pool_in_weight,
    query_weight,
    forget_weight,
    input_weight,
    forget_gap,
    decay_shift,
    out_gain,
    pool_out_weight,
    recur_out_weight,
):
    pool_cols = pool_in_weight.shape[1]
    recur_cols = query_weight.shape[1]
    local_in = jnp.concatenate([pool_in_weight, query_weight, forget_weight, input_weight], axis=1)
    whole_in = lax.all_gather(local_in, "sp", axis=0, tiled=True)
    floats = tokens.astype(jnp.float32)
    scale = lax.rsqrt(jnp.mean(floats * floats, axis=-1, keepdims=True) + EPSILON)
    normed = (floats * scale * norm_gain).astype(jnp.bfloat16)
    pool_weight = whole_in[:, :pool_cols]
    recur_weight = whole_in[:, pool_cols:]
    pooled_in = jnp.dot(
        lax.all_gather(normed, "tp", axis=0, tiled=True),
        pool_weight,
        preferred_element_type=jnp.float32,
    ).astype(jnp.bfloat16)
    recur_in = jnp.dot(
        lax.all_gather(normed, "tp", axis=0, tiled=True),
        recur_weight,
        preferred_element_type=jnp.float32,
    ).astype(jnp.bfloat16)
    query = recur_in[:, :recur_cols].astype(jnp.float32)
    forget_pre = recur_in[:, recur_cols : 2 * recur_cols].astype(jnp.float32)
    values = recur_in[:, 2 * recur_cols :].astype(jnp.float32)
    row_count = pooled_in.shape[0]
    head_count = recur_cols // RDIM
    block_count = row_count // SPAN
    gate_pre = forget_pre.reshape(row_count, head_count, RDIM)
    opened = forget_gap.reshape(head_count, RDIM) * jax.nn.sigmoid(-gate_pre)
    log_decay = jnp.log1p(-opened) + decay_shift.T[:, :, None]
    query_blocks = to_blocks(query, block_count, head_count)
    decay_blocks = to_blocks(log_decay, block_count, head_count)
    key_blocks = to_blocks(opened, block_count, head_count)
    value_blocks = to_blocks(values, block_count, head_count)
    causal = jnp.tril(jnp.ones((SPAN, SPAN), jnp.bool_))
    inner_block_output = jnp.cumsum(decay_blocks, axis=2)
    block_decay_total = inner_block_output[:, :, -1, :]
    decayed_query = query_blocks * jnp.exp(inner_block_output)
    scores = jnp.einsum(
        "bhtk,bhsk->bhts",
        decayed_query,
        key_blocks * jnp.exp(-inner_block_output),
        precision=EXACT_MATMUL,
    )
    scores = jnp.where(causal, scores, 0.0)
    received_output = jnp.einsum("bhts,bhsv->bhtv", scores, value_blocks, precision=EXACT_MATMUL)
    growth_factor = jnp.einsum(
        "bhsk,bhsv->bhkv",
        key_blocks * jnp.exp(block_decay_total[:, :, None, :] - inner_block_output),
        value_blocks,
        precision=EXACT_MATMUL,
    )
    fading = jnp.exp(block_decay_total)

    def carry_step(state_matrix, item):
        return (item[0][:, :, None] * state_matrix + item[1], state_matrix)

    empty_state = jnp.zeros((head_count, RDIM, RDIM), jnp.float32)
    local_state, block_starts = lax.scan(carry_step, empty_state, (fading, growth_factor))
    received_output = received_output + jnp.einsum(
        "bhtk,bhkv->bhtv", decayed_query, block_starts, precision=EXACT_MATMUL
    )
    earlier_total = jnp.cumsum(block_decay_total, axis=0) - block_decay_total
    decay_from_start = query_blocks * jnp.exp(inner_block_output + earlier_total[:, :, None, :])
    device_fade = jnp.exp(jnp.sum(block_decay_total, axis=0))
    reach = 2**GROUPS - 1
    rim = pooled_in[row_count - reach :]
    unit_fade = jnp.ones((head_count, RDIM), jnp.float32)
    previous = passed_along(rim, "sp", 1)
    carried_fade, carried_state = prefix(
        (device_fade, local_state), "sp", chain, (unit_fade, empty_state)
    )
    received_output = received_output + jnp.einsum(
        "fuoy,uyi->fuoi", decay_from_start, carried_state, precision=EXACT_MATMUL
    )
    received_output = received_output.transpose(0, 2, 1, 3).reshape(row_count, head_count, RDIM)
    spread = lax.rsqrt(
        jnp.mean(received_output * received_output, axis=-1, keepdims=True) + EPSILON
    )
    recur_mixed = (
        (received_output * spread * out_gain).astype(jnp.bfloat16).reshape(row_count, recur_cols)
    )
    group = lax.axis_index("tp")
    padded = jnp.concatenate([previous, pooled_in], axis=0).astype(jnp.float32)
    results = window_sums(padded, GROUPS, reach)
    window_sum = results[GROUPS - 1]
    for level in range(GROUPS - 1):
        window_sum = jnp.where(group == level, results[level], window_sum)
    width = jnp.left_shift(jnp.int32(2), group)
    position = lax.axis_index("sp") * row_count + jnp.arange(row_count, dtype=jnp.int32)
    divisor = jnp.minimum(position + 1, width).astype(jnp.float32)[:, None]
    pool_mixed = (window_sum / divisor - pooled_in.astype(jnp.float32)).astype(jnp.bfloat16)
    out_pool, out_recur = (
        lax.all_gather(pool_out_weight, "sp", axis=1, tiled=True),
        lax.all_gather(recur_out_weight, "sp", axis=1, tiled=True),
    )
    partial_value = jnp.dot(pool_mixed, out_pool, preferred_element_type=jnp.float32)
    return lax.psum_scatter(
        (
            partial_value + jnp.dot(recur_mixed, out_recur, preferred_element_type=jnp.float32)
        ).astype(jnp.bfloat16),
        "tp",
        scatter_dimension=0,
        tiled=True,
    )


def solution(mesh):
    in_specs = (
        P(("sp", "tp"), None),
        P(),
        P("sp", "tp"),
        P("sp", "tp"),
        P("sp", "tp"),
        P("sp", "tp"),
        P("tp"),
        P("tp", "sp"),
        P(),
        P("tp", "sp"),
        P("tp", "sp"),
    )
    out_specs = P(("sp", "tp"), None)
    return jax.shard_map(local, mesh=mesh, in_specs=in_specs, out_specs=out_specs, check_vma=False)
```

profile of v0, /device:TPU:0, one launch (start us, length us, event | category | flops | bytes accessed | tf_op | source)
XLA Modules:
  0.0 273.9 jit_solution(6150586459145285040)
XLA Ops:
  6.5 1.3 fusion.7
  7.8 2.0 fusion.9
  9.9 2.0 pad_maximum_fusion
  11.9 0.7 all-gather.13.cloned.1.call-update
  12.9 22.4 %all-gather.9.cloned.1.call-done = bf16[512,2048]{1,0:T(8,128)(2,1)} async-done(((bf16[128,2048]{1,0:T(8,128)(2,1)}), bf16[512,2048]{1,0:T(8,128)(2,1)}) %all-gather.9.cloned.1.call-update) | async-done | bytes 2097168 | tf_op jit(solution)/shard_map/all_gather | solution.py:75
  35.3 74.9 %all-gather.11.cloned.1.call-done = bf16[2048,1024]{1,0:T(8,128)(2,1)} async-done(((bf16[256,1024]{1,0:T(8,128)(2,1)}), bf16[2048,1024]{1,0:T(8,128)(2,1)}) %all-gather.11.cloned.1.call-update) | async-done | bytes 4194320 | tf_op jit(solution)/shard_map/all_gather | solution.py:68
  110.2 4.3 %fusion.2 = bf16[512,768]{1,0:T(8,128)(2,1)S(1)} fusion(bf16[512,2048]{1,0:T(8,128)(2,1)} %all-gather.9.cloned.1.call-done, bf16[2048,1024]{1,0:T(8,128)(2,1)} %all-gather.11.cloned.1.call-done), kind=kOutput, calls=%fused_computation.8 | convolution fusion | flops 1611005952 | bytes 6029312 | tf_op jit(solution)/shard_map/dot_general | solution.py:79
  116.2 1.5 bitcast_multiply_fusion.4
  117.7 1.0 fusion.21
  118.7 6.6 %while.26 = (s32[]{:T(128)}, f32[2,128,128]{2,1,0:T(8,128)S(1)}, f32[8,2,128,128]{3,2,1,0:T(8,128)}, f32[8,2,128]{2,0,1:T(8,128)S(1)}, f32[8,2,128,128]{3,2,1,0:T(8,128)S(1)}, /*index=5*/s32[]{:T(128)}, s32[]{:T(128)}) while((s32[]{:T(128)}, f32[2,128,128]{2,1,0:T(8,128)S(1)}, f32[8,2,128,128]{3,2,1,0:T(8,128)}, ...), condition=%wide.region_3.4_spmd.clone, body=%wide.region_2.3_spmd.clone.sunk | while | flops 131075 | bytes 658540 | solution.py:121
  118.7 0.7 bitcast_dynamic-update-slice_fusion.2
  119.6 0.7 bitcast_dynamic-update-slice_fusion.2
  120.4 0.7 bitcast_dynamic-update-slice_fusion.2
  121.2 0.7 bitcast_dynamic-update-slice_fusion.2
  122.0 0.7 bitcast_dynamic-update-slice_fusion.2
  122.9 0.7 bitcast_dynamic-update-slice_fusion.2
  123.7 0.7 bitcast_dynamic-update-slice_fusion.2
  124.5 0.7 bitcast_dynamic-update-slice_fusion.2
  125.3 0.6 copy-done.1
  126.0 0.5 all-gather.15.cloned.1.call-update
  126.7 2.6 convolution_convert_fusion
  129.3 2.5 collective-permute-start
  131.8 1.2 convolution_select_fusion
  133.4 18.6 %all-gather.2 = f32[8,2,128]{2,1,0:T(2,128)S(1)} all-gather(f32[1,2,128]{2,1,0:T(2,128)S(1)} %exponential_bitcast_fusion), channel_id=2, replica_groups=mesh['sp'=8,'tp'=4] {'sp'}, dimensions={0}, use_global_device_ids=true | all-gather | bytes 9216 | tf_op jit(solution)/shard_map/all_gather | solution.py:21
  152.3 4.1 %fusion.30 = f32[512,2048]{1,0:T(8,128)} fusion(bf16[256,2048]{1,0:T(8,128)(2,1)} %all-gather.13.cloned.1.call-done, bf16[512,256]{1,0:T(8,128)(2,1)S(1)} %convolution_convert_fusion, f32[520,256]{1,0:T(8,128)S(1)} %slice_add_fusion.2, f32[526,256]{1,0:T(8,128)S(1)} %slice_add_fusion.1, f32[524,256]{1,0:T(8,128)S(1)} %slice_add_fusion, ...), kind=kOutput, calls=%fused_computation.54 | convolution fusion | flops 537919488 | bytes 7604227 | tf_op jit(solution)/shard_map/dot_general | solution.py:159
  156.3 35.2 %all-gather.17.cloned.1.call-done = f32[16,128,128]{2,1,0:T(8,128)} async-done(((f32[2,128,128]{2,1,0:T(8,128)}), f32[16,128,128]{2,1,0:T(8,128)}) %all-gather.17.cloned.1.call-update) | async-done | bytes 1048592 | tf_op jit(solution)/shard_map/all_gather | solution.py:21
  191.7 0.7 convolution_bitcast_fusion
  192.4 2.6 multiply_reduce_fusion
  195.6 36.0 %all-gather.15.cloned.1.call-done = bf16[256,2048]{1,0:T(8,128)(2,1)} async-done(((bf16[256,256]{1,0:T(8,128)(2,1)}), bf16[256,2048]{1,0:T(8,128)(2,1)}) %all-gather.15.cloned.1.call-update) | async-done | bytes 1048592 | tf_op jit(solution)/shard_map/all_gather | solution.py:157
  231.5 0.6 mul.113
  232.1 4.6 %add_convert_fusion = bf16[512,2048]{1,0:T(8,128)(2,1)} fusion(f32[512,2048]{1,0:T(8,128)} %fusion.30, bf16[256,2048]{1,0:T(8,128)(2,1)} %all-gather.15.cloned.1.call-done, f32[64,8,2,128]{3,2,1,0:T(2,128)S(1)} %bitcast.79, f32[64,8,2,128]{3,2,1,0:T(2,128)S(1)} %bitcast.78, f32[256]{0:T(256)S(1)} %broadcast_bitcast_fusion), kind=kOutput, calls=%fused_computation.5 | convolution fusion | flops 539361280 | bytes 8389632 | tf_op jit(solution)/shard_map/dot_general | solution.py:162
  236.7 30.3 %reduce-scatter.2.cloned.1.call-done = bf16[128,2048]{1,0:T(8,128)(2,1)} async-done(((bf16[512,2048]{1,0:T(8,128)(2,1)}), bf16[128,2048]{1,0:T(8,128)(2,1)}) %reduce-scatter.2.cloned.1.call-update) | async-done | bytes 524304 | tf_op jit(solution)/shard_map/reduce_scatter | solution.py:160
  (67 shorter events, 4.4 us)
Async XLA Ops:
  6.5 120.1 %copy-start = (f32[128]{0:T(128)S(1)}, f32[128]{0:T(128)}, u32[]{:S(2)}) copy-start(f32[128]{0:T(128)} %param.23) | copy-start | bytes 1540
  6.5 6.2 %copy-start.3 = (f32[2,512]{1,0:T(2,128)S(1)}, f32[2,512]{1,0:T(2,128)}, u32[]{:S(2)}) copy-start(f32[2,512]{1,0:T(2,128)} %param.22) | copy-start | bytes 12292
  6.5 28.8 %all-gather.9.cloned.1.call-start = ((), (), s32[]{:S(2)}) async-start(), calls=%async_computation.1 | async-start | bytes 2621440 | tf_op jit(solution)/shard_map/all_gather | solution.py:75
  9.9 100.4 %all-gather.11.cloned.1.call-start = ((), (), s32[]{:S(2)}) async-start(), calls=%async_computation.2 | async-start | bytes 4718592 | tf_op jit(solution)/shard_map/all_gather | solution.py:68
  11.9 140.4 %all-gather.13.cloned.1.call-start = ((), (), s32[]{:S(2)}) async-start(), calls=%async_computation.3 | async-start | bytes 1179648 | tf_op jit(solution)/shard_map/all_gather | solution.py:156
  12.6 178.9 %all-gather.17.cloned.1.call-start = ((), (), s32[]{:S(2)}) async-start(), calls=%async_computation.6 | async-start | bytes 1179648 | tf_op jit(solution)/shard_map/all_gather | solution.py:21
  114.6 0.7 copy-start.4
  125.3 0.7 copy-start.1
  126.0 105.5 %all-gather.15.cloned.1.call-start = ((), (), s32[]{:S(2)}) async-start(), calls=%async_computation.4 | async-start | bytes 1179648 | tf_op jit(solution)/shard_map/all_gather | solution.py:157
  126.6 140.5 %reduce-scatter.2.cloned.1.call-start = ((), (), s32[]{:S(2)}) async-start(), calls=%async_computation.5 | async-start | bytes 2621440 | tf_op jit(solution)/shard_map/reduce_scatter | solution.py:160
  129.3 22.7 %collective-permute-start = (bf16[15,256]{1,0:T(8,128)(2,1)S(1)}, bf16[15,256]{1,0:T(8,128)(2,1)S(1)}, u32[]{:S(2)}, u32[]{:S(2)}) collective-permute-start(bf16[15,256]{1,0:T(8,128)(2,1)S(1)} %slice.70), channel_id=1, source_target_pairs={{0,4},{4,8},{8,12},{12,16},{16,20},{20,24},{24,28},{1,5},{5,9},{9,... | collective-permute-start | bytes 23048 | tf_op jit(solution)/shard_map/ppermute | solution.py:16
  152.2 39.5 %copy-start.2 = (f32[8,2,64,128]{3,0,1,2:T(8,128)S(1)}, f32[8,2,64,128]{3,0,1,2:T(8,128)}, u32[]{:S(2)}) copy-start(f32[8,2,64,128]{3,0,1,2:T(8,128)} %get-tuple-element.146) | copy-start | bytes 1572868
Sparse Core Ops, SparseCore 0:
  10.0 25.2 all-gather.8
  37.4 72.7 all-gather.10
  112.3 37.9 all-gather.12
  152.2 39.1 all-gather.16
  193.4 38.0 all-gather.14
  236.8 30.1 reduce-scatter.1
where the time goes:
time: 274 us
  waiting for transfers between devices  200 us (73%)
  matrix products  21.4 us (8%)
  blocking collectives  18.6 us (7%)
  other arithmetic  14 us (5%)
  between operations  13.8 us (5%)
  local copies, waits for them, and re-layouts  2.88 us (1%)
    all_gather x1, waiting for transfers between devices, local(): whole_in = lax.all_gather(local_in, 'sp', axis=0, tiled=True)  74.9 us
    all_gather x1, waiting for transfers between devices, local(): lax.all_gather(recur_out_weight, 'sp', axis=1, tiled=True)  36 us
    all_gather x1, waiting for transfers between devices, prefix(): gathered = jax.tree.map(lambda a: lax.all_gather(a, axis), part)  35.2 us
    reduce_scatter x1, waiting for transfers between devices, local(): lax.psum_scatter((partial_value + jnp.dot(recur_mixed, out_recur, preferr...  30.3 us
    all_gather x1, waiting for transfers between devices, local(): lax.all_gather(normed, 'tp', axis=0, tiled=True)  22.4 us
    all_gather x1, blocking collectives, prefix(): gathered = jax.tree.map(lambda a: lax.all_gather(a, axis), part)  18.6 us
  transfers between devices with their start and end apart: 7, of which 5 were waited for; matrix products, arithmetic and copies ran while one was open for 11% of the time, Pallas kernels for 0%

commit v1 on v0

--- a/solution.py
+++ b/solution.py
@@ -152,9 +152,15 @@
     position = lax.axis_index("sp") * row_count + jnp.arange(row_count, dtype=jnp.int32)
     divisor = jnp.minimum(position + 1, width).astype(jnp.float32)[:, None]
     pool_mixed = (window_sum / divisor - pooled_in.astype(jnp.float32)).astype(jnp.bfloat16)
+    sizes_cut = lambda matrix, axis_no, axis_tag: jnp.concatenate(
+        lax.all_to_all(
+            jnp.stack([matrix for _ in range(lax.axis_size(axis_tag))], axis=0), axis_tag, 0, 0
+        ),
+        axis=axis_no,
+    )
     out_pool, out_recur = (
         lax.all_gather(pool_out_weight, "sp", axis=1, tiled=True),
-        lax.all_gather(recur_out_weight, "sp", axis=1, tiled=True),
+        sizes_cut(recur_out_weight, 1, "sp"),
     )
     partial_value = jnp.dot(pool_mixed, out_pool, preferred_element_type=jnp.float32)
     return lax.psum_scatter(

time: 274 us -> 245 us (0.89)
  waiting for transfers between devices: 200 us -> 150 us
  local copies, waits for them, and re-layouts: 2.88 us -> 11.4 us
  starting transfers between devices: 2.66 us -> 10.4 us
  other arithmetic: 14 us -> 18.5 us
    all_gather x1 -> x0, waiting for transfers between devices: 36 us -> none  [local(): lax.all_gather(recur_out_weight, 'sp', axis=1, tiled=True)]
    all_gather x1, waiting for transfers between devices: 35.2 us -> 24.1 us  [prefix(): gathered = jax.tree.map(lambda a: lax.all_gather(a, axis), part)]
    all_gather x1, waiting for transfers between devices: 22.4 us -> 12.7 us  [local(): lax.all_gather(normed, 'tp', axis=0, tiled=True)]
    all_to_all x0 -> x1, starting transfers between devices: none -> 7.28 us  [local(): lax.all_to_all(jnp.stack([matrix for _ in range(lax.axis_size(axis_tag))]...]
    reduce_scatter x1, waiting for transfers between devices: 30.3 us -> 37.5 us  [local(): lax.psum_scatter((partial_value + jnp.dot(recur_mixed, out_recur, preferr...]
    dynamic_slice x8, local copies, waits for them, and re-layouts: 0.06 us -> 5.65 us  [local(): lax.scan(carry_step, empty_state, (fading, growth_factor))]
  transfers between devices with their start and end apart: 7 -> 7, of which waited for: 5 -> 4; matrix products, arithmetic and copies ran while one was open for 11% -> 18% of each run, Pallas kernels for 0% -> 0%
where the time goes in v1:
time: 245 us; the launch traced here: 244 us
  waiting for transfers between devices  150 us (61%)
  matrix products  21.6 us (9%)
  other arithmetic  18.5 us (8%)
  blocking collectives  17.8 us (7%)
  between operations  13.5 us (6%)
  local copies, waits for them, and re-layouts  11.4 us (5%)
  starting transfers between devices  10.4 us (4%)
    all_gather x1, waiting for transfers between devices, local(): whole_in = lax.all_gather(local_in, 'sp', axis=0, tiled=True)  74.9 us
    reduce_scatter x1, waiting for transfers between devices, local(): lax.psum_scatter((partial_value + jnp.dot(recur_mixed, out_recur, preferr...  37.5 us
    all_gather x1, waiting for transfers between devices, prefix(): gathered = jax.tree.map(lambda a: lax.all_gather(a, axis), part)  24.1 us
    all_gather x1, blocking collectives, prefix(): gathered = jax.tree.map(lambda a: lax.all_gather(a, axis), part)  17.8 us
    all_gather x1, waiting for transfers between devices, local(): lax.all_gather(normed, 'tp', axis=0, tiled=True)  12.7 us
    all_to_all x1, starting transfers between devices, local(): lax.all_to_all(jnp.stack([matrix for _ in range(lax.axis_size(axis_tag))]...  7.28 us
    dynamic_slice x8, local copies, waits for them, and re-layouts, local(): lax.scan(carry_step, empty_state, (fading, growth_factor))  5.65 us
    dynamic_update_slice x8, other arithmetic, local(): lax.scan(carry_step, empty_state, (fading, growth_factor))  5.28 us
  transfers between devices with their start and end apart: 7, of which 4 were waited for; matrix products, arithmetic and copies ran while one was open for 18% of the time, Pallas kernels for 0%

profile of v1, /device:TPU:0, one launch (start us, length us, event | category | flops | bytes accessed | tf_op | source)
XLA Modules:
  0.0 243.7 jit_solution(14772320486867762685)
XLA Ops:
  6.5 1.3 fusion.7
  7.8 2.0 fusion.9
  9.9 2.0 pad_maximum_fusion
  12.0 1.1 stack.2
  13.1 7.3 %all-to-all-start = ((bf16[8,256,256]{1,2,0:T(8,128)(2,1)}), bf16[8,256,256]{1,2,0:T(8,128)(2,1)S(1)}, u32[]{:S(2)}, u32[]{:S(2)}) async-start(bf16[8,256,256]{1,2,0:T(8,128)(2,1)} %stack.2), calls=%async_computation | async-start | bytes 2097152 | tf_op jit(solution)/shard_map/all_to_all | solution.py:156
  21.3 0.7 copy.34
  22.6 12.7 %all-gather.8.cloned.1.call-done = bf16[512,2048]{1,0:T(8,128)(2,1)} async-done(((bf16[128,2048]{1,0:T(8,128)(2,1)}), bf16[512,2048]{1,0:T(8,128)(2,1)}) %all-gather.8.cloned.1.call-update) | async-done | bytes 2097168 | tf_op jit(solution)/shard_map/all_gather | solution.py:75
  35.3 74.9 %all-gather.10.cloned.1.call-done = bf16[2048,1024]{1,0:T(8,128)(2,1)} async-done(((bf16[256,1024]{1,0:T(8,128)(2,1)}), bf16[2048,1024]{1,0:T(8,128)(2,1)}) %all-gather.10.cloned.1.call-update) | async-done | bytes 4194320 | tf_op jit(solution)/shard_map/all_gather | solution.py:68
  110.3 4.3 %fusion.2 = bf16[512,768]{1,0:T(8,128)(2,1)S(1)} fusion(bf16[512,2048]{1,0:T(8,128)(2,1)} %all-gather.8.cloned.1.call-done, bf16[2048,1024]{1,0:T(8,128)(2,1)} %all-gather.10.cloned.1.call-done), kind=kOutput, calls=%fused_computation.8 | convolution fusion | flops 1611005952 | bytes 6029312 | tf_op jit(solution)/shard_map/dot_general | solution.py:79
  115.2 1.3 fusion.16
  117.2 2.6 %convolution_convert_fusion = bf16[512,256]{1,0:T(8,128)(2,1)S(1)} fusion(bf16[512,2048]{1,0:T(8,128)(2,1)} %all-gather.8.cloned.1.call-done, bf16[2048,1024]{1,0:T(8,128)(2,1)} %all-gather.10.cloned.1.call-done), kind=kOutput, calls=%fused_computation.16 | convolution fusion | flops 537001984 | bytes 3407872 | tf_op jit(solution)/shard_map/dot_general | solution.py:74
  120.5 3.0 %collective-permute-start = (bf16[15,256]{1,0:T(8,128)(2,1)}, bf16[15,256]{1,0:T(8,128)(2,1)}, u32[]{:S(2)}, u32[]{:S(2)}) collective-permute-start(bf16[15,256]{1,0:T(8,128)(2,1)} %slice.70), channel_id=1, source_target_pairs={{0,4},{4,8},{8,12},{12,16},{16,20},{20,24},{24,28},{1,5},{5,9},{9,... | collective-permute-start | bytes 23048 | tf_op jit(solution)/shard_map/ppermute | solution.py:16
  123.6 1.2 slice_bitcast_fusion
  124.7 1.1 reshape.90
  125.8 2.6 %bitcast_multiply_fusion.3 = (f32[8,2,64,128]{3,0,1,2:T(8,128)S(1)}, f32[8,2,64,128]{3,0,1,2:T(8,128)}, f32[8,2,64,128]{3,0,1,2:T(8,128)S(1)}, f32[8,2,64,128]{3,0,1,2:T(8,128)S(1)}) fusion(f32[8,2,64,128]{3,0,1,2:T(8,128)S(1)} %fusion.16, f32[8,64,2,128]{3,2,1,0:T(2,128)} %reshape.90, f32[8,2,128]{2,0,1:T(8,128)} %get-tuple-element.143, ...), kind=kLoop, calls=%fused_computation.36 | loop fusion | flops 1048576 | bytes 3687424 | tf_op jit(solution)/shard_map/mul | solution.py:100
  128.4 1.0 fusion.19
  129.4 12.1 %while.26 = (s32[]{:T(128)}, f32[2,128,128]{2,1,0:T(8,128)S(1)}, f32[8,2,128,128]{3,2,1,0:T(8,128)}, f32[8,2,128]{2,0,1:T(8,128)}, f32[8,2,128,128]{3,2,1,0:T(8,128)S(1)}, /*index=5*/s32[]{:T(128)}, s32[]{:T(128)}) while((s32[]{:T(128)}, f32[2,128,128]{2,1,0:T(8,128)S(1)}, f32[8,2,128,128]{3,2,1,0:T(8,128)}, ...), condition=%wide.region_3.4_spmd.clone, body=%wide.region_2.3_spmd.clone.sunk | while | flops 131075 | bytes 658540 | solution.py:121
  129.5 0.7 constant_dynamic-slice_fusion.2
  131.0 0.7 constant_dynamic-slice_fusion.2
  134.0 0.7 constant_dynamic-slice_fusion.2
  135.5 0.7 constant_dynamic-slice_fusion.2
  140.0 0.7 constant_dynamic-slice_fusion.2
  142.3 1.2 convolution_select_fusion
  143.5 1.2 fusion.33
  144.7 17.8 %all-gather.2 = f32[8,2,128]{2,1,0:T(2,128)S(1)} all-gather(f32[1,2,128]{2,1,0:T(2,128)S(1)} %exponential_bitcast_fusion), channel_id=2, replica_groups=mesh['sp'=8,'tp'=4] {'sp'}, dimensions={0}, use_global_device_ids=true | all-gather | bytes 9216 | tf_op jit(solution)/shard_map/all_gather | solution.py:21
  162.5 0.8 maximum_convert_fusion
  163.5 4.0 %fusion.28 = f32[512,2048]{1,0:T(8,128)} fusion(bf16[256,2048]{1,0:T(8,128)(2,1)} %all-gather.12.cloned.1.call-done, bf16[512,256]{1,0:T(8,128)(2,1)S(1)} %copy-done.3, f32[520,256]{1,0:T(8,128)S(1)} %slice_add_fusion.2, f32[526,256]{1,0:T(8,128)S(1)} %slice_add_fusion.1, f32[524,256]{1,0:T(8,128)S(1)} %slice_add_fusion, f32[512]{0:T(512)S(1)} %copy-done.6, ...), kind=kOutput, calls=%fused_computation.52 | convolution fusion | flops 537919488 | bytes 7604227 | tf_op jit(solution)/shard_map/dot_general | solution.py:165
  167.5 24.1 %all-gather.14.cloned.1.call-done = f32[16,128,128]{2,1,0:T(8,128)} async-done(((f32[2,128,128]{2,1,0:T(8,128)}), f32[16,128,128]{2,1,0:T(8,128)}) %all-gather.14.cloned.1.call-update) | async-done | bytes 1048592 | tf_op jit(solution)/shard_map/all_gather | solution.py:21
  191.8 1.7 convolution_bitcast_fusion
  193.6 1.3 multiply_reduce_fusion
  195.3 4.3 %add_convert_fusion = bf16[512,2048]{1,0:T(8,128)(2,1)} fusion(f32[512,2048]{1,0:T(8,128)} %fusion.28, bf16[256,2048]{0,1:T(8,128)(2,1)S(1)} %bitcast.70, bf16[64,8,2,128]{3,2,1,0:T(2,128)(2,1)S(1)} %bitcast.71), kind=kOutput, calls=%fused_computation.5 | convolution fusion | flops 538968064 | bytes 7602176 | tf_op jit(solution)/shard_map/dot_general | solution.py:168
  199.7 37.5 %reduce-scatter.2.cloned.1.call-done = bf16[128,2048]{1,0:T(8,128)(2,1)} async-done(((bf16[512,2048]{1,0:T(8,128)(2,1)}), bf16[128,2048]{1,0:T(8,128)(2,1)}) %reduce-scatter.2.cloned.1.call-update) | async-done | bytes 524304 | tf_op jit(solution)/shard_map/reduce_scatter | solution.py:166
  (78 shorter events, 13.5 us)
Async XLA Ops:
  6.5 5.4 %copy-start.5 = (bf16[256,256]{1,0:T(8,128)(2,1)S(1)}, bf16[256,256]{1,0:T(8,128)(2,1)}, u32[]{:S(2)}) copy-start(bf16[256,256]{1,0:T(8,128)(2,1)} %param.25) | copy-start | bytes 393220
  6.5 28.8 %all-gather.8.cloned.1.call-start = ((), (), s32[]{:S(2)}) async-start(), calls=%async_computation.2 | async-start | bytes 2621440 | tf_op jit(solution)/shard_map/all_gather | solution.py:75
  9.8 11.4 %copy-start.7 = (f32[2,512]{1,0:T(2,128)S(1)}, f32[2,512]{1,0:T(2,128)}, u32[]{:S(2)}) copy-start(f32[2,512]{1,0:T(2,128)} %param.22) | copy-start | bytes 12292
  9.9 100.4 %all-gather.10.cloned.1.call-start = ((), (), s32[]{:S(2)}) async-start(), calls=%async_computation.3 | async-start | bytes 4718592 | tf_op jit(solution)/shard_map/all_gather | solution.py:68
  13.1 182.2 %all-to-all-start = ((bf16[8,256,256]{1,2,0:T(8,128)(2,1)}), bf16[8,256,256]{1,2,0:T(8,128)(2,1)S(1)}, u32[]{:S(2)}, u32[]{:S(2)}) async-start(bf16[8,256,256]{1,2,0:T(8,128)(2,1)} %stack.2), calls=%async_computation | async-start | bytes 2097152 | tf_op jit(solution)/shard_map/all_to_all | solution.py:156
  20.4 143.1 %all-gather.12.cloned.1.call-start = ((), (), s32[]{:S(2)}) async-start(), calls=%async_computation.4 | async-start | bytes 1179648 | tf_op jit(solution)/shard_map/all_gather | solution.py:162
  21.1 170.5 %all-gather.14.cloned.1.call-start = ((), (), s32[]{:S(2)}) async-start(), calls=%async_computation.6 | async-start | bytes 1179648 | tf_op jit(solution)/shard_map/all_gather | solution.py:21
  114.6 0.7 copy-start.9
  119.8 3.6 %copy-start.2 = (bf16[512,256]{1,0:T(8,128)(2,1)}, bf16[512,256]{1,0:T(8,128)(2,1)S(1)}, u32[]{:S(2)}) copy-start(bf16[512,256]{1,0:T(8,128)(2,1)S(1)} %convolution_convert_fusion) | copy-start | bytes 786436
  120.5 42.0 %collective-permute-start = (bf16[15,256]{1,0:T(8,128)(2,1)}, bf16[15,256]{1,0:T(8,128)(2,1)}, u32[]{:S(2)}, u32[]{:S(2)}) collective-permute-start(bf16[15,256]{1,0:T(8,128)(2,1)} %slice.70), channel_id=1, source_target_pairs={{0,4},{4,8},{8,12},{12,16},{16,20},{20,24},{24,28},{1,5},{5,9},{9,... | collective-permute-start | bytes 23048 | tf_op jit(solution)/shard_map/ppermute | solution.py:16
  129.4 15.2 %copy-start.8 = (f32[2,128]{1,0:T(2,128)S(1)}, f32[2,128]{1,0:T(2,128)}, u32[]{:S(2)}) copy-start(f32[2,128]{1,0:T(2,128)} %get-tuple-element.142) | copy-start | bytes 3076
  141.5 0.7 copy-start
  141.5 21.0 %copy-start.3 = (bf16[512,256]{1,0:T(8,128)(2,1)S(1)}, bf16[512,256]{1,0:T(8,128)(2,1)}, u32[]{:S(2)}) copy-start(bf16[512,256]{1,0:T(8,128)(2,1)} %copy-done.2) | copy-start | bytes 786436
  142.2 95.0 %reduce-scatter.2.cloned.1.call-start = ((), (), s32[]{:S(2)}) async-start(), calls=%async_computation.5 | async-start | bytes 2621440 | tf_op jit(solution)/shard_map/reduce_scatter | solution.py:166
  144.6 18.8 %copy-start.6 = (f32[512]{0:T(512)S(1)}, f32[512]{0:T(512)}, u32[]{:S(2)}) copy-start(f32[512]{0:T(512)} %minimum_convert_fusion) | copy-start | bytes 6148
  167.5 26.0 %copy-start.1 = (f32[8,2,64,128]{3,2,1,0:T(8,128)S(1)}, f32[8,2,64,128]{3,2,1,0:T(8,128)}, u32[]{:S(2)}) copy-start(f32[8,2,64,128]{3,2,1,0:T(8,128)} %fusion.33) | copy-start | bytes 1572868
  167.5 26.0 %copy-start.4 = (f32[8,2,128,128]{3,2,1,0:T(8,128)S(1)}, f32[8,2,128,128]{3,2,1,0:T(8,128)}, u32[]{:S(2)}) copy-start(f32[8,2,128,128]{3,2,1,0:T(8,128)} %get-tuple-element.77) | copy-start | bytes 3145732
  191.6 3.2 %copy-start.10 = (f32[128]{0:T(128)S(1)}, f32[128]{0:T(128)}, u32[]{:S(2)}) copy-start(f32[128]{0:T(128)} %param.23) | copy-start | bytes 1540
Sparse Core Ops, SparseCore 0:
  10.0 25.2 all-gather.7
  37.4 72.7 all-gather.9
  112.3 37.9 all-gather.11
  152.3 39.2 all-gather.13
  199.8 37.3 reduce-scatter.1
